TPU v7x, 32 devices: a whole 2x2x4 slice. The times are simulated.
32 devices in a mesh: sp: 16 (over z, y, x), tp: 2 (over core).
Axes of the slice: x: 2, y: 2, z: 4, core: 2. Of those that a mesh axis runs over, the one named last changes fastest.
Arguments:
- gate_pre: bfloat16 [4096, 2048], P('sp', 'tp'), may hold values from -6 to 6
- conv_in: bfloat16 [4096, 2048], P('sp', 'tp'), may hold values from -6 to 6
- conv_taps: bfloat16 [4, 2048], P(None, 'tp'), may hold values from -3 to 3
- recur_map: bfloat16 [8, 256, 256], P('tp'), may hold values from -0.375 to 0.375
- input_map: bfloat16 [8, 256, 256], P('tp'), may hold values from -0.375 to 0.375
- rate_logit: float32 [2048], P('tp'), may hold values from 4.5 to 15
- decay_shift: float32 [4096, 8], P('sp', 'tp'), may hold values from -1.5 to 0
- out_weight: bfloat16 [2048, 2048], replicated, may hold values from -0.25 to 0.25
- residual: bfloat16 [4096, 2048], P(('sp', 'tp')), may hold values from -6 to 6
- gain_mix: float32 [2048], replicated, may hold values from 0.1 to 1.9
- routes: int32 [4096, 4], P(('sp', 'tp')), may hold values from 0 to 31, all different within a row; in each aligned block of 128 rows (0 to 127, 128 to 255, ...) at most 32 rows name the same one
- route_weight: float32 [4096, 4], P(('sp', 'tp')), may hold values from 0.2 to 1
- shared_gate: bfloat16 [2048, 512], replicated, may hold values from -0.125 to 0.125
- shared_up: bfloat16 [2048, 512], replicated, may hold values from -0.125 to 0.125
- shared_down: bfloat16 [512, 2048], replicated, may hold values from -0.375 to 0.375
- expert_gate: bfloat16 [32, 2048, 512], P(('sp', 'tp')), may hold values from -0.125 to 0.125
- expert_up: bfloat16 [32, 2048, 512], P(('sp', 'tp')), may hold values from -0.125 to 0.125
- expert_down: bfloat16 [32, 512, 2048], P(('sp', 'tp')), may hold values from -0.375 to 0.375
- gain_out: float32 [2048], replicated, may hold values from 0.1 to 1.9
Outputs:
- layer_out: bfloat16 [4096, 2048], P(('sp', 'tp'))
Inputs may be any that keep to these rules, and one draw needn't show every extreme that they name: `routes`: each row names 4 different experts. In the rows of one device (aligned blocks of 128 rows) no expert is named more than 32 times, and in some blocks one expert is named exactly 32 times.
All inputs are finite; a program needn't handle non-finite values.
Results may differ from a plain program's by a relative error of at most 0.014.
Values may be sent and summed in bfloat16 or wider, within the bound.
A program may use at most 128 MiB of HBM per device.

v0:
```python
import jax
import jax.numpy as jnp
from jax import lax
from jax.sharding import PartitionSpec as P

ALPHA = 8.0**0.25
RATE_C = 8.0
NORM_EPS = 1e-05


def from_behind(block, axis, distance):
    devices = range(lax.axis_size(axis))
    route = [(i - distance, i) for i in devices if i - distance in devices]
    return lax.ppermute(block, axis, route)


def entering(value, axis, join, neutral):
    count, mine = (lax.axis_size(axis), lax.axis_index(axis))
    pieces = jax.tree.map(lambda part: lax.all_gather(part, axis), value)
    subtotal = jax.tree.map(
        lambda part, zero: jnp.full_like(part, 0) + jnp.asarray(zero, part.dtype), value, neutral
    )

    def turn(position, subtotal):
        longer = join(subtotal, jax.tree.map(lambda part: part[position], pieces))
        return jax.tree.map(lambda new, old: jnp.where(position < mine, new, old), longer, subtotal)

    return lax.fori_loop(0, count - 1, turn, subtotal)


def layer_norm(values, gains):
    center = values - jnp.mean(values, axis=-1, keepdims=True)
    spread = jnp.mean(center * center, axis=-1, keepdims=True)
    return center * lax.rsqrt(spread + NORM_EPS) * gains


def combine(former, latter):
    return (former[0] * latter[0], latter[0] * former[1] + latter[1])


def on_device(
    gate_pre,
    conv_in,
    conv_taps,
    recur_map,
    input_map,
    rate_logit,
    decay_shift,
    out_weight,
    residual,
    gain_mix,
    routes,
    route_weight,
    shared_gate,
    shared_up,
    shared_down,
    expert_gate,
    expert_up,
    expert_down,
    gain_out,
):
    tokens, channels = conv_in.shape
    reach = conv_taps.shape[0] - 1
    head_count, head_width = (recur_map.shape[0], recur_map.shape[1])
    before = from_behind(conv_in[tokens - reach :], "sp", 1)
    extended = jnp.concatenate([before, conv_in], axis=0).astype(jnp.float32)
    filter_tap_weight = conv_taps.astype(jnp.float32)
    summed = jnp.zeros((tokens, channels), jnp.float32)
    for offset in range(reach + 1):
        summed = summed + filter_tap_weight[offset] * extended[offset : offset + tokens]
    conv_out = summed.astype(jnp.bfloat16).reshape(tokens, head_count, head_width)
    recur_gate = jax.nn.sigmoid(
        jnp.einsum("thc,hcd->thd", conv_out, recur_map, preferred_element_type=jnp.float32)
    )
    input_gate = jax.nn.sigmoid(
        jnp.einsum("thc,hcd->thd", conv_out, input_map, preferred_element_type=jnp.float32)
    )
    log_decay = (
        -RATE_C * jax.nn.softplus(-rate_logit).reshape(head_count, head_width) * recur_gate
        + decay_shift[:, :, None]
    )
    update = jnp.sqrt(-jnp.expm1(2.0 * log_decay)) * input_gate * conv_out.astype(jnp.float32)
    running, local_state = lax.associative_scan(combine, (jnp.exp(log_decay), update), axis=0)
    carried = entering(
        (running[-1], local_state[-1]),
        "sp",
        combine,
        (jnp.ones_like(running[-1]), jnp.zeros_like(local_state[-1])),
    )
    states = local_state + running * carried[1][None]
    mixed_rows = (
        states.reshape(tokens, channels)
        * jax.nn.gelu(gate_pre.astype(jnp.float32), approximate=True)
    ).astype(jnp.bfloat16)
    row_count = tokens // lax.axis_size("tp")
    regrouped = lax.all_to_all(mixed_rows, "tp", split_axis=0, concat_axis=1, tiled=True)
    projected = jnp.dot(regrouped, out_weight, preferred_element_type=jnp.float32)
    normed = layer_norm(ALPHA * residual.astype(jnp.float32) + projected, gain_mix).astype(
        jnp.bfloat16
    )
    model_width = normed.shape[1]
    fanout = routes.shape[1]
    sp_count, tp_count = (lax.axis_size("sp"), lax.axis_size("tp"))
    experts = sp_count * tp_count
    capacity = max(2, 2 * row_count * fanout // experts)
    entries = row_count * fanout
    flat_ids = routes.reshape(entries)
    onehot = (flat_ids[:, None] == lax.iota(jnp.int32, experts)[None, :]).astype(jnp.bfloat16)
    before_mask = (
        lax.iota(jnp.int32, entries)[:, None] > lax.iota(jnp.int32, entries)[None, :]
    ).astype(jnp.bfloat16)
    earlier = jnp.dot(before_mask, onehot, preferred_element_type=jnp.float32)
    slot_rank = jnp.sum(earlier * onehot.astype(jnp.float32), axis=1).astype(jnp.int32)
    slot_index = flat_ids * capacity + slot_rank
    source_row = (
        jnp.full((experts * capacity,), row_count, jnp.int32)
        .at[slot_index]
        .set(lax.iota(jnp.int32, entries) // fanout)
    )
    padded_rows = jnp.concatenate([normed, jnp.zeros((1, model_width), jnp.bfloat16)], axis=0)
    outgoing = padded_rows[source_row].reshape(experts, capacity, model_width)
    shared_hidden = (
        jax.nn.silu(jnp.dot(normed, shared_gate, preferred_element_type=jnp.float32))
        * jnp.dot(normed, shared_up, preferred_element_type=jnp.float32)
    ).astype(jnp.bfloat16)
    shared_out = jnp.dot(shared_hidden, shared_down, preferred_element_type=jnp.float32)
    received = lax.all_to_all(outgoing, ("sp", "tp"), split_axis=0, concat_axis=0, tiled=True)
    senders = received.shape[0]
    slot_count = received.shape[1]
    chosen = received.reshape(senders * slot_count, model_width)
    hidden = (
        jax.nn.silu(jnp.dot(chosen, expert_gate[0], preferred_element_type=jnp.float32))
        * jnp.dot(chosen, expert_up[0], preferred_element_type=jnp.float32)
    ).astype(jnp.bfloat16)
    handed_result = lax.all_to_all(
        jnp.dot(hidden, expert_down[0], preferred_element_type=jnp.float32)
        .astype(jnp.bfloat16)
        .reshape(senders, slot_count, model_width),
        ("sp", "tp"),
        split_axis=0,
        concat_axis=0,
        tiled=True,
    )
    gathered = handed_result.reshape(experts * capacity, model_width)[slot_index].reshape(
        row_count, fanout, model_width
    )
    moe_sum = shared_out + jnp.sum(route_weight[:, :, None] * gathered.astype(jnp.float32), axis=1)
    return layer_norm(ALPHA * normed.astype(jnp.float32) + moe_sum, gain_out).astype(jnp.bfloat16)


def solution(mesh):
    return jax.shard_map(
        on_device,
        mesh=mesh,
        in_specs=(
            P("sp", "tp"),
            P("sp", "tp"),
            P(None, "tp"),
            P("tp", None, None),
            P("tp", None, None),
            P("tp"),
            P("sp", "tp"),
            P(),
            P(("sp", "tp"), None),
            P(),
            P(("sp", "tp"), None),
            P(("sp", "tp"), None),
            P(),
            P(),
            P(),
            P(("sp", "tp"), None, None),
            P(("sp", "tp"), None, None),
            P(("sp", "tp"), None, None),
            P(),
        ),
        out_specs=P(("sp", "tp"), None),
        check_vma=False,
    )
```

profile of v0, /device:TPU:0, one launch (start us, length us, event | category | flops | bytes accessed | tf_op | source)
XLA Modules:
  0.0 477.8 jit_solution(17262271969213903551)
XLA Ops:
  1.8 4.9 %collective-permute-start = (bf16[3,1024]{0,1:T(8,128)(2,1)}, bf16[3,1024]{0,1:T(8,128)(2,1)S(1)}, u32[]{:S(2)}, u32[]{:S(2)}) collective-permute-start(bf16[3,1024]{0,1:T(8,128)(2,1)} %copy.36), channel_id=1, source_target_pairs={{0,2},{2,4},{4,6},{6,8},{8,10},{10,12},{12,14},{14,16},{16,18},{18... | collective-permute-start | bytes 18440 | tf_op jit(solution)/shard_map/ppermute | solution.py:14
  10.3 2.4 scatter_custom_fusion
  20.8 2.0 fusion.14
  22.8 3.3 slice.275
  26.1 3.2 slice.276
  94.5 3.3 slice.330
  97.8 3.3 slice.273
  112.4 4.3 pad.114
  118.3 3.8 pad.127
  122.1 2.2 pad.128
  124.4 2.1 add.327
  126.4 2.5 fusion.36
  129.8 4.3 pad.113
  134.9 39.5 %all_gather.7 = f32[16,4,256]{2,1,0:T(4,128)S(1)} all-gather(f32[1,4,256]{2,1,0:T(4,128)S(1)} %copy.42), channel_id=1, replica_groups=mesh['sp'=16,'tp'=2] {'sp'}, dimensions={0}, use_global_device_ids=true | all-gather | bytes 69632 | tf_op jit(solution)/shard_map/all_gather | solution.py:19
  174.4 4.3 pad.130
  180.6 4.3 pad.129
  185.7 35.8 %all_gather.6 = f32[16,4,256]{2,1,0:T(4,128)S(1)} all-gather(f32[1,4,256]{2,1,0:T(4,128)S(1)} %copy.41), channel_id=1, replica_groups=mesh['sp'=16,'tp'=2] {'sp'}, dimensions={0}, use_global_device_ids=true | all-gather | bytes 69632 | tf_op jit(solution)/shard_map/all_gather | solution.py:19
  222.0 3.1 multiply_add_fusion
  228.2 4.2 all_to_all.29
  232.4 4.8 fusion.67
  237.7 6.0 %gather_fusion = bf16[1024,2048]{1,0:T(8,128)(2,1)} fusion(bf16[129,2048]{1,0:T(8,128)(2,1)S(1)} %concatenate.63, s32[1024]{0:T(1024)S(1)} %fusion.55), kind=kCustom, calls=%fused_computation | custom fusion | bytes 8392704 | tf_op jit(solution)/shard_map/gather | solution.py:121
  243.7 96.5 %all_to_all.30 = bf16[32,32,2048]{2,1,0:T(8,128)(2,1)S(1)} all-to-all(bf16[32,32,2048]{2,1,0:T(8,128)(2,1)} %bitcast.81), channel_id=1, replica_groups=mesh['sp'=16,'tp'=2] {'sp','tp'}, dimensions={0} | all-to-all | bytes 8388608 | tf_op jit(solution)/shard_map/all_to_all | solution.py:127
  340.3 2.0 copy-done.3
  342.3 3.7 fusion.3
  345.9 10.1 %convolution_convert_fusion = bf16[1024,2048]{1,0:T(8,128)(2,1)} fusion(bf16[1,512,2048]{2,1,0:T(8,128)(2,1)S(1)} %copy-done, f32[1024,512]{1,0:T(8,128)} %fusion.3, bf16[1024,2048]{1,0:T(8,128)(2,1)} %bitcast.84, bf16[1,2048,512]{2,1,0:T(8,128)(2,1)} %param.36), kind=kOutput, calls=%fused_computation.7 | convolution fusion | flops 4300210176 | bytes 14680064 | tf_op jit(solution)/shard_map/dot_general | solution.py:136
  356.0 3.9 all-to-all-start.2
  360.1 2.0 fusion.69
  362.2 91.5 %all-to-all-done.2 = bf16[32,32,2048]{2,1,0:T(8,128)(2,1)} async-done(((bf16[32,32,2048]{2,1,0:T(8,128)(2,1)}), bf16[32,32,2048]{2,1,0:T(8,128)(2,1)}, u32[]{:S(2)}, u32[]{:S(2)}) %all-to-all-start.2) | async-done | bytes 4194336 | tf_op jit(solution)/shard_map/all_to_all | solution.py:135
  453.7 8.0 %gather_fusion.1 = bf16[512,2048]{1,0:T(8,128)(2,1)} fusion(bf16[1024,2048]{1,0:T(8,128)(2,1)} %bitcast.18, s32[1024]{0:T(1024)S(1)} %pad_clamp_fusion), kind=kCustom, calls=%fused_computation.1 | custom fusion | bytes 4196352 | tf_op jit(solution)/shard_map/gather | solution.py:144
  461.6 4.8 reshape.101
  466.4 6.4 %multiply_reduce_fusion = f32[128,2048]{1,0:T(8,128)} fusion(f32[128,4,2048]{2,1,0:T(4,128)} %reshape.101, f32[128,4]{1,0:T(8,128)S(1)} %copy.46), kind=kLoop, calls=%fused_computation.6 | loop fusion | flops 1835008 | bytes 5244928 | tf_op jit(solution)/shard_map/reduce_sum | solution.py:147
  472.7 3.8 fusion.68
  (245 shorter events, 101.1 us)
Async XLA Ops:
  0.0 345.9 %copy-start = (bf16[1,512,2048]{2,1,0:T(8,128)(2,1)S(1)}, bf16[1,512,2048]{2,1,0:T(8,128)(2,1)}, u32[]{:S(2)}) copy-start(bf16[1,512,2048]{2,1,0:T(8,128)(2,1)} %param.38) | copy-start | bytes 6291460
  0.0 14.1 %copy-start.8 = (bf16[256,1024]{1,0:T(8,128)(2,1)S(1)}, bf16[256,1024]{1,0:T(8,128)(2,1)}, u32[]{:S(2)}) copy-start(bf16[256,1024]{1,0:T(8,128)(2,1)} %param.21) | copy-start | bytes 1572868
  1.8 13.3 %collective-permute-start = (bf16[3,1024]{0,1:T(8,128)(2,1)}, bf16[3,1024]{0,1:T(8,128)(2,1)S(1)}, u32[]{:S(2)}, u32[]{:S(2)}) collective-permute-start(bf16[3,1024]{0,1:T(8,128)(2,1)} %copy.36), channel_id=1, source_target_pairs={{0,2},{2,4},{4,6},{6,8},{8,10},{10,12},{12,14},{14,16},{16,18},{18... | collective-permute-start | bytes 18440 | tf_op jit(solution)/shard_map/ppermute | solution.py:14
  10.3 5.1 %copy-start.34 = (s32[512,1]{0,1:T(1,128)}, s32[512,1]{0,1:T(1,128)S(1)}, u32[]{:S(2)}) copy-start(s32[512,1]{0,1:T(1,128)S(1)} %compare_select_fusion) | copy-start | bytes 6148
  15.5 3.4 copy-start.39
  20.8 10.0 %copy-start.4 = (f32[256,4,256]{2,0,1:T(8,128)}, f32[256,4,256]{2,0,1:T(8,128)S(1)}, u32[]{:S(2)}) copy-start(f32[256,4,256]{2,0,1:T(8,128)S(1)} %get-tuple-element.176) | copy-start | bytes 3145732
  91.7 12.1 %copy-start.17 = (f32[2,4,256]{2,0,1:T(2,128)S(1)}, f32[2,4,256]{2,0,1:T(2,128)}, u32[]{:S(2)}) copy-start(f32[2,4,256]{2,0,1:T(2,128)} %get-tuple-element.183) | copy-start | bytes 24580
  91.7 12.2 %copy-start.28 = (f32[1,4,256]{2,0,1:T(1,128)S(1)}, f32[1,4,256]{2,0,1:T(1,128)}, u32[]{:S(2)}) copy-start(f32[1,4,256]{2,0,1:T(1,128)} %get-tuple-element.160) | copy-start | bytes 12292
  91.7 12.2 %copy-start.29 = (f32[1,4,256]{2,0,1:T(1,128)S(1)}, f32[1,4,256]{2,0,1:T(1,128)}, u32[]{:S(2)}) copy-start(f32[1,4,256]{2,0,1:T(1,128)} %get-tuple-element.161) | copy-start | bytes 12292
  91.7 12.2 %copy-start.30 = (f32[1,4,256]{2,0,1:T(1,128)S(1)}, f32[1,4,256]{2,0,1:T(1,128)}, u32[]{:S(2)}) copy-start(f32[1,4,256]{2,0,1:T(1,128)} %get-tuple-element.162) | copy-start | bytes 12292
  91.7 12.2 %copy-start.31 = (f32[1,4,256]{2,0,1:T(1,128)S(1)}, f32[1,4,256]{2,0,1:T(1,128)}, u32[]{:S(2)}) copy-start(f32[1,4,256]{2,0,1:T(1,128)} %get-tuple-element.163) | copy-start | bytes 12292
  91.7 12.7 %copy-start.13 = (f32[7,4,256]{2,0,1:T(8,128)S(1)}, f32[7,4,256]{2,0,1:T(8,128)}, u32[]{:S(2)}) copy-start(f32[7,4,256]{2,0,1:T(8,128)} %slice.297) | copy-start | bytes 86020
  91.7 12.7 %copy-start.14 = (f32[7,4,256]{2,0,1:T(8,128)S(1)}, f32[7,4,256]{2,0,1:T(8,128)}, u32[]{:S(2)}) copy-start(f32[7,4,256]{2,0,1:T(8,128)} %slice.322) | copy-start | bytes 86020
  93.3 12.7 %copy-start.11 = (f32[15,4,256]{2,0,1:T(8,128)S(1)}, f32[15,4,256]{2,0,1:T(8,128)}, u32[]{:S(2)}) copy-start(f32[15,4,256]{2,0,1:T(8,128)} %slice.291) | copy-start | bytes 184324
  93.3 12.7 %copy-start.12 = (f32[15,4,256]{2,0,1:T(8,128)S(1)}, f32[15,4,256]{2,0,1:T(8,128)}, u32[]{:S(2)}) copy-start(f32[15,4,256]{2,0,1:T(8,128)} %slice.324) | copy-start | bytes 184324
  93.9 10.2 %copy-start.15 = (f32[3,4,256]{2,0,1:T(4,128)S(1)}, f32[3,4,256]{2,0,1:T(4,128)}, u32[]{:S(2)}) copy-start(f32[3,4,256]{2,0,1:T(4,128)} %slice.303) | copy-start | bytes 36868
  93.9 10.2 %copy-start.16 = (f32[3,4,256]{2,0,1:T(4,128)S(1)}, f32[3,4,256]{2,0,1:T(4,128)}, u32[]{:S(2)}) copy-start(f32[3,4,256]{2,0,1:T(4,128)} %slice.320) | copy-start | bytes 36868
  93.9 10.2 %copy-start.27 = (f32[1,4,256]{2,0,1:T(1,128)S(1)}, f32[1,4,256]{2,0,1:T(1,128)}, u32[]{:S(2)}) copy-start(f32[1,4,256]{2,0,1:T(1,128)} %slice.391) | copy-start | bytes 12292
  93.9 10.3 %copy-start.26 = (f32[1,4,256]{2,0,1:T(1,128)S(1)}, f32[1,4,256]{2,0,1:T(1,128)}, u32[]{:S(2)}) copy-start(f32[1,4,256]{2,0,1:T(1,128)} %slice.365) | copy-start | bytes 12292
  94.5 11.6 %copy-start.25 = (f32[1,4,256]{2,0,1:T(1,128)S(1)}, f32[1,4,256]{2,0,1:T(1,128)}, u32[]{:S(2)}) copy-start(f32[1,4,256]{2,0,1:T(1,128)} %slice.389) | copy-start | bytes 12292
  97.8 8.4 %copy-start.24 = (f32[1,4,256]{2,0,1:T(1,128)S(1)}, f32[1,4,256]{2,0,1:T(1,128)}, u32[]{:S(2)}) copy-start(f32[1,4,256]{2,0,1:T(1,128)} %slice.363) | copy-start | bytes 12292
  109.7 7.0 %copy-start.20 = (f32[1,4,256]{2,0,1:T(1,128)S(1)}, f32[1,4,256]{2,0,1:T(1,128)}, u32[]{:S(2)}) copy-start(f32[1,4,256]{2,0,1:T(1,128)} %slice.387) | copy-start | bytes 12292
  129.0 5.2 %copy-start.2 = (f32[256,4,256]{2,0,1:T(8,128)S(1)}, f32[256,4,256]{2,0,1:T(8,128)}, u32[]{:S(2)}) copy-start(f32[256,4,256]{2,0,1:T(8,128)} %pad.114) | copy-start | bytes 3145732
  129.0 49.8 %copy-start.18 = (f32[1,4,256]{2,0,1:T(1,128)S(1)}, f32[1,4,256]{2,0,1:T(1,128)}, u32[]{:S(2)}) copy-start(f32[1,4,256]{2,0,1:T(1,128)} %slice.386) | copy-start | bytes 12292
  226.7 5.7 %copy-start.7 = (bf16[128,2048]{1,0:T(8,128)(2,1)S(1)}, bf16[128,2048]{1,0:T(8,128)(2,1)}, u32[]{:S(2)}) copy-start(bf16[128,2048]{1,0:T(8,128)(2,1)} %param.29) | copy-start | bytes 1572868
  232.4 5.0 %copy-start.32 = (f32[2048]{0:T(1024)S(1)}, f32[2048]{0:T(1024)}, u32[]{:S(2)}) copy-start(f32[2048]{0:T(1024)} %param.30) | copy-start | bytes 24580
  237.7 122.5 %copy-start.1 = (bf16[128,2048]{1,0:T(8,128)(2,1)}, bf16[128,2048]{1,0:T(8,128)(2,1)S(1)}, u32[]{:S(2)}) copy-start(bf16[128,2048]{1,0:T(8,128)(2,1)S(1)} %multiply_convert_fusion.2) | copy-start | bytes 1572868
  243.7 98.5 %copy-start.37 = (bf16[1,2048,512]{2,1,0:T(8,128)(2,1)S(1)}, bf16[1,2048,512]{2,1,0:T(8,128)(2,1)}, u32[]{:S(2)}) copy-start(bf16[1,2048,512]{2,1,0:T(8,128)(2,1)} %param.37) | copy-start | bytes 6291460
  356.0 4.0 copy-start.36
  356.0 4.1 copy-start.35
  356.0 97.6 %all-to-all-start.2 = ((bf16[32,32,2048]{2,1,0:T(8,128)(2,1)}), bf16[32,32,2048]{2,1,0:T(8,128)(2,1)}, u32[]{:S(2)}, u32[]{:S(2)}) async-start(bf16[32,32,2048]{2,1,0:T(8,128)(2,1)} %bitcast.82), calls=%async_computation.2 | async-start | bytes 8388608 | tf_op jit(solution)/shard_map/all_to_all | solution.py:135
  472.7 4.1 copy-start.33
  (10 other events, 18.3 us)
where the time goes:
time: 482 us; the launch traced here: 478 us
  blocking collectives  176 us (37%)
  local copies, waits for them, and re-layouts  127 us (26%)
  waiting for transfers between devices  91.5 us (19%)
  other arithmetic  44.6 us (9%)
  matrix products  28.5 us (6%)
  starting transfers between devices  8.82 us (2%)
    all_to_all x1, blocking collectives, on_device(): lax.all_to_all(outgoing, ('sp', 'tp'), split_axis=0, concat_axis=0, tiled...  96.5 us
    all_to_all x1, waiting for transfers between devices, on_device(): lax.all_to_all(jnp.dot(hidden, expert_down[0], preferred_element_type=jnp...  91.5 us
    all_gather x2, blocking collectives, entering(): pieces = jax.tree.map(lambda part: lax.all_gather(part, axis), value)  75.3 us
    slice x52, local copies, waits for them, and re-layouts, on_device(): lax.associative_scan(combine, (jnp.exp(log_decay), update), axis=0)  68.2 us
    pad x28, local copies, waits for them, and re-layouts, on_device(): lax.associative_scan(combine, (jnp.exp(log_decay), update), axis=0)  26.1 us
    add x13, other arithmetic, combine(): return (former[0] * latter[0], latter[0] * former[1] + latter[1])  15 us
    dot_general x1, matrix products, on_device(): jnp.dot(hidden, expert_down[0], preferred_element_type=jnp.float32)  10.1 us
  transfers between devices with their start and end apart: 2, of which 1 were waited for; matrix products, arithmetic and copies ran while one was open for 2% of the time, Pallas kernels for 0%

commit v1 on v0

--- a/solution.py
+++ b/solution.py
@@ -1,11 +1,16 @@
+import functools
+
 import jax
 import jax.numpy as jnp
 from jax import lax
+from jax.experimental import pallas as pl
+from jax.experimental.pallas import tpu as pltpu
 from jax.sharding import PartitionSpec as P
 
 ALPHA = 8.0**0.25
 RATE_C = 8.0
 NORM_EPS = 1e-05
+MESH = pl.DeviceIdType.MESH
 
 
 def from_behind(block, axis, distance):
@@ -14,28 +19,134 @@
     return lax.ppermute(block, axis, route)
 
 
-def entering(value, axis, join, neutral):
-    count, mine = (lax.axis_size(axis), lax.axis_index(axis))
-    pieces = jax.tree.map(lambda part: lax.all_gather(part, axis), value)
-    subtotal = jax.tree.map(
-        lambda part, zero: jnp.full_like(part, 0) + jnp.asarray(zero, part.dtype), value, neutral
-    )
-
-    def turn(position, subtotal):
-        longer = join(subtotal, jax.tree.map(lambda part: part[position], pieces))
-        return jax.tree.map(lambda new, old: jnp.where(position < mine, new, old), longer, subtotal)
-
-    return lax.fori_loop(0, count - 1, turn, subtotal)
+def expm1_of_negative(y):
+    series = jnp.ones_like(y)
+    for order in range(8, 1, -1):
+        series = 1.0 + series * y * (1.0 / order)
+    return jnp.where(y > -0.35, y * series, jnp.exp(y) - 1.0)
+
+
+def recurrence_kernel(
+    before_ref, conv_ref, taps_ref, recur_ref, input_ref, coef_ref, shift_ref, run_ref, state_ref, tail_ref
+):
+    tokens, width = conv_ref.shape
+    reach = taps_ref.shape[0] - 1
+    x = conv_ref[...].astype(jnp.float32)
+    before = before_ref[...]
+    taps = taps_ref[...].astype(jnp.float32)
+    top_row = lax.broadcasted_iota(jnp.int32, (8, width), 0)
+    summed = jnp.zeros((tokens, width), jnp.float32)
+    for offset in range(reach + 1):
+        back = reach - offset
+        if back:
+            moved = pltpu.roll(x, back, 0)
+            first = jnp.where(top_row < back, pltpu.roll(before, back, 0), moved[:8])
+            moved = jnp.concatenate([first, moved[8:]], axis=0)
+        else:
+            moved = x
+        summed = summed + taps[offset : offset + 1] * moved
+    conv_out = summed.astype(jnp.bfloat16)
+    recur_gate = jax.nn.sigmoid(jnp.dot(conv_out, recur_ref[0], preferred_element_type=jnp.float32))
+    input_gate = jax.nn.sigmoid(jnp.dot(conv_out, input_ref[0], preferred_element_type=jnp.float32))
+    shifts = shift_ref[...]
+    column = lax.broadcasted_iota(jnp.int32, shifts.shape, 1)
+    shift = jnp.sum(jnp.where(column == pl.program_id(0), shifts, 0.0), axis=1, keepdims=True)
+    log_decay = coef_ref[...] * recur_gate + shift
+    update = jnp.sqrt(-expm1_of_negative(2.0 * log_decay)) * input_gate * conv_out.astype(jnp.float32)
+    run, state = jnp.exp(log_decay), update
+    row = lax.broadcasted_iota(jnp.int32, (tokens, width), 0)
+    step = 1
+    while step < tokens:
+        if step < 8:
+            inside = row >= step
+            run_before = jnp.where(inside, pltpu.roll(run, step, 0), 1.0)
+            state_before = jnp.where(inside, pltpu.roll(state, step, 0), 0.0)
+        else:
+            run_before = jnp.concatenate([jnp.ones((step, width), jnp.float32), run[:-step]], axis=0)
+            state_before = jnp.concatenate([jnp.zeros((step, width), jnp.float32), state[:-step]], axis=0)
+        state = state + run * state_before
+        run = run * run_before
+        step *= 2
+    run_ref[...] = run
+    state_ref[...] = state
+    tail_ref[...] = jnp.where(top_row == 7, run[tokens - 8 :], pltpu.roll(state[tokens - 8 :], 7, 0))
+
+
+def recurrence(before, conv_in, conv_taps, recur_map, input_map, coef, decay_shift):
+    tokens, channels = conv_in.shape
+    heads, width = recur_map.shape[:2]
+    return pl.pallas_call(
+        recurrence_kernel,
+        grid=(heads,),
+        in_specs=[
+            pl.BlockSpec((8, width), lambda h: (0, h)),
+            pl.BlockSpec((tokens, width), lambda h: (0, h)),
+            pl.BlockSpec((conv_taps.shape[0], width), lambda h: (0, h)),
+            pl.BlockSpec((1, width, width), lambda h: (h, 0, 0)),
+            pl.BlockSpec((1, width, width), lambda h: (h, 0, 0)),
+            pl.BlockSpec((1, width), lambda h: (0, h)),
+            pl.BlockSpec((tokens, heads), lambda h: (0, 0)),
+        ],
+        out_specs=[
+            pl.BlockSpec((tokens, width), lambda h: (0, h)),
+            pl.BlockSpec((tokens, width), lambda h: (0, h)),
+            pl.BlockSpec((8, width), lambda h: (0, h)),
+        ],
+        out_shape=[
+            jax.ShapeDtypeStruct((tokens, channels), jnp.float32),
+            jax.ShapeDtypeStruct((tokens, channels), jnp.float32),
+            jax.ShapeDtypeStruct((8, channels), jnp.float32),
+        ],
+    )(before, conv_in, conv_taps, recur_map, input_map, coef, decay_shift)
+
+
+def entering_kernel(count, tail_ref, out_ref, land, send_sem, recv_sem):
+    me, core = lax.axis_index("sp"), lax.axis_index("tp")
+    barrier = pltpu.get_barrier_semaphore()
+    for d in range(1, count):
+        pl.semaphore_signal(barrier, inc=1, device_id=(lax.rem(me + d, count), core), device_id_type=MESH)
+    pl.semaphore_wait(barrier, count - 1)
+    copies = []
+    for d in range(1, count):
+        copy = pltpu.make_async_remote_copy(
+            src_ref=tail_ref,
+            dst_ref=land.at[d],
+            send_sem=send_sem.at[d],
+            recv_sem=recv_sem.at[d],
+            device_id=(lax.rem(me + d, count), core),
+            device_id_type=MESH,
+        )
+        copy.start()
+        copies.append(copy)
+    for copy in copies:
+        copy.wait()
+    carry = jnp.zeros((1, tail_ref.shape[1]), jnp.float32)
+    for d in range(count - 1, 0, -1):
+        longer = land[d, 7:8] * carry + land[d, 6:7]
+        carry = jnp.where(jnp.full(carry.shape, d, jnp.int32) <= me, longer, carry)
+    out_ref[...] = carry
+
+
+def entering(tail):
+    count = lax.axis_size("sp")
+    return pl.pallas_call(
+        functools.partial(entering_kernel, count),
+        out_shape=jax.ShapeDtypeStruct((1, tail.shape[1]), jnp.float32),
+        in_specs=[pl.BlockSpec(memory_space=pltpu.VMEM)],
+        out_specs=pl.BlockSpec(memory_space=pltpu.VMEM),
+        scratch_shapes=[
+            pltpu.VMEM((count, *tail.shape), jnp.float32),
+            pltpu.SemaphoreType.DMA((count,)),
+            pltpu.SemaphoreType.DMA((count,)),
+        ],
+        compiler_params=pltpu.CompilerParams(collective_id=0, has_side_effects=True),
+    )(tail)
 
 
 def layer_norm(values, gains):
     center = values - jnp.mean(values, axis=-1, keepdims=True)
     spread = jnp.mean(center * center, axis=-1, keepdims=True)
     return center * lax.rsqrt(spread + NORM_EPS) * gains
-
-
-def combine(former, latter):
-    return (former[0] * latter[0], latter[0] * former[1] + latter[1])
 
 
 def on_device(
@@ -61,37 +172,14 @@
 ):
     tokens, channels = conv_in.shape
     reach = conv_taps.shape[0] - 1
-    head_count, head_width = (recur_map.shape[0], recur_map.shape[1])
-    before = from_behind(conv_in[tokens - reach :], "sp", 1)
-    extended = jnp.concatenate([before, conv_in], axis=0).astype(jnp.float32)
-    filter_tap_weight = conv_taps.astype(jnp.float32)
-    summed = jnp.zeros((tokens, channels), jnp.float32)
-    for offset in range(reach + 1):
-        summed = summed + filter_tap_weight[offset] * extended[offset : offset + tokens]
-    conv_out = summed.astype(jnp.bfloat16).reshape(tokens, head_count, head_width)
-    recur_gate = jax.nn.sigmoid(
-        jnp.einsum("thc,hcd->thd", conv_out, recur_map, preferred_element_type=jnp.float32)
-    )
-    input_gate = jax.nn.sigmoid(
-        jnp.einsum("thc,hcd->thd", conv_out, input_map, preferred_element_type=jnp.float32)
-    )
-    log_decay = (
-        -RATE_C * jax.nn.softplus(-rate_logit).reshape(head_count, head_width) * recur_gate
-        + decay_shift[:, :, None]
-    )
-    update = jnp.sqrt(-jnp.expm1(2.0 * log_decay)) * input_gate * conv_out.astype(jnp.float32)
-    running, local_state = lax.associative_scan(combine, (jnp.exp(log_decay), update), axis=0)
-    carried = entering(
-        (running[-1], local_state[-1]),
-        "sp",
-        combine,
-        (jnp.ones_like(running[-1]), jnp.zeros_like(local_state[-1])),
-    )
-    states = local_state + running * carried[1][None]
-    mixed_rows = (
-        states.reshape(tokens, channels)
-        * jax.nn.gelu(gate_pre.astype(jnp.float32), approximate=True)
-    ).astype(jnp.bfloat16)
+    before = from_behind(conv_in[tokens - reach :], "sp", 1).astype(jnp.float32)
+    before = jnp.concatenate([jnp.zeros((8 - reach, channels), jnp.float32), before], axis=0)
+    coef = (-RATE_C * jax.nn.softplus(-rate_logit)).reshape(1, channels)
+    running, local_state, tail = recurrence(
+        before, conv_in, conv_taps, recur_map, input_map, coef, decay_shift
+    )
+    states = local_state + running * entering(tail)
+    mixed_rows = (states * jax.nn.gelu(gate_pre.astype(jnp.float32), approximate=True)).astype(jnp.bfloat16)
     row_count = tokens // lax.axis_size("tp")
     regrouped = lax.all_to_all(mixed_rows, "tp", split_axis=0, concat_axis=1, tiled=True)
     projected = jnp.dot(regrouped, out_weight, preferred_element_type=jnp.float32)

time: 482 us -> 293 us (0.61)
  local copies, waits for them, and re-layouts: 127 us -> 27.1 us
  blocking collectives: 176 us -> 106 us
  other arithmetic: 44.6 us -> 12.7 us
  Pallas kernels: 0 us -> 20.8 us
    all_gather x2 -> x0, blocking collectives: 75.3 us -> none  [entering(): pieces = jax.tree.map(lambda part: lax.all_gather(part, axis), value)]
    slice x57 -> x1, local copies, waits for them, and re-layouts: 70.8 us -> 0.88 us  [on_device(): before = from_behind(conv_in[tokens - reach:], 'sp', 1).astype(jnp.float32)]
    pad x28 -> x0, local copies, waits for them, and re-layouts: 26.1 us -> none  [on_device(): lax.associative_scan(combine, (jnp.exp(log_decay), update), axis=0)]
    add x29 -> x0, other arithmetic: 24.1 us -> none  [the longest x13 15 us: combine(): return (former[0] * latter[0], latter[0] * former[1] + latter[1])]
    pallas_call x0 -> x2, Pallas kernels: none -> 20.8 us  [the longest x1 14.3 us: entering(): pl.pallas_call(functools.partial(entering_kernel, count), out_shape=jax.S...]
    all_to_all x1, blocking collectives: 96.5 us -> 102 us  [on_device(): lax.all_to_all(outgoing, ('sp', 'tp'), split_axis=0, concat_axis=0, tiled...]
    concatenate x13 -> x1, other arithmetic: 5.93 us -> 0.62 us  [on_device(): jnp.concatenate([jnp.zeros((8 - reach, channels), jnp.float32), before],...]
  transfers between devices with their start and end apart: 2 -> 2, of which waited for: 1 -> 1; matrix products, arithmetic and copies ran while one was open for 2% -> 3% of each run, Pallas kernels for 0% -> 0%
where the time goes in v1:
time: 293 us; the launch traced here: 292 us
  blocking collectives  106 us (36%)
  waiting for transfers between devices  91.5 us (31%)
  local copies, waits for them, and re-layouts  27.1 us (9%)
  matrix products  24.7 us (8%)
  Pallas kernels  20.8 us (7%)
  other arithmetic  12.7 us (4%)
  starting transfers between devices  8.83 us (3%)
    all_to_all x1, blocking collectives, on_device(): lax.all_to_all(outgoing, ('sp', 'tp'), split_axis=0, concat_axis=0, tiled...  102 us
    all_to_all x1, waiting for transfers between devices, on_device(): lax.all_to_all(jnp.dot(hidden, expert_down[0], preferred_element_type=jnp...  91.5 us
    pallas_call x1, Pallas kernels, entering(): pl.pallas_call(functools.partial(entering_kernel, count), out_shape=jax.S...  14.3 us
    dot_general x1, matrix products, on_device(): jnp.dot(hidden, expert_down[0], preferred_element_type=jnp.float32)  10.1 us
    gather x1, local copies, waits for them, and re-layouts, on_device(): handed_result.reshape(experts * capacity, model_width)[slot_index]  7.96 us
    pallas_call x1, Pallas kernels, recurrence(): pl.pallas_call(recurrence_kernel, grid=(heads,), in_specs=[pl.BlockSpec((...  6.44 us
    reduce_sum x1, other arithmetic, on_device(): jnp.sum(route_weight[:, :, None] * gathered.astype(jnp.float32), axis=1)  6.33 us
    gather x1, local copies, waits for them, and re-layouts, on_device(): outgoing = padded_rows[source_row].reshape(experts, capacity, model_width)  6.02 us
  transfers between devices with their start and end apart: 2, of which 1 were waited for; matrix products, arithmetic and copies ran while one was open for 3% of the time, Pallas kernels for 0%

profile of v1, /device:TPU:0, one launch (start us, length us, event | category | flops | bytes accessed | tf_op | source)
XLA Modules:
  0.0 292.2 jit_solution(16059492105913014562)
XLA Ops:
  0.0 0.9 slice.3
  0.9 4.9 %collective-permute-start = (bf16[3,1024]{1,0:T(4,128)(2,1)S(1)}, bf16[3,1024]{1,0:T(4,128)(2,1)S(1)}, u32[]{:S(2)}, u32[]{:S(2)}) collective-permute-start(bf16[3,1024]{1,0:T(4,128)(2,1)S(1)} %slice.3), channel_id=1, source_target_pairs={{0,2},{2,4},{4,6},{6,8},{8,10},{10,12},{12,14},{14,16},{16,18},{18... | collective-permute-start | bytes 18440 | tf_op jit(solution)/shard_map/ppermute | solution.py:19
  5.8 0.8 copy.26
  6.5 0.7 broadcast_multiply_fusion
  7.2 1.3 fusion.27
  8.6 0.3 fusion.9
  8.9 0.1 copy.25
  9.2 2.4 scatter_custom_fusion
  11.6 1.5 copy.22.shift_ref
  13.1 0.6 pad_convert_fusion.before_ref
  13.7 6.4 %shard_map.181 = (f32[256,1024]{1,0:T(8,128)}, f32[256,1024]{1,0:T(8,128)}, f32[8,1024]{1,0:T(8,128)}) custom-call(f32[8,1024]{1,0:T(8,128)} %pad_convert_fusion.before_ref, bf16[256,1024]{1,0:T(8,128)(2,1)} %conv_ref.1, bf16[4,1024]{1,0:T(4,128)(2,1)} %taps_ref.1, bf16[4,256,256]{2,1,0:T(8,128)(2,1)} %recur_ref.1, bf16[4,256,256]{2,1,0:T(8,128)(2,1)} %input_ref.1, ...), custom_call_target="tpu_custom_call" | custom-call | tf_op jit(solution)/shard_map/pallas_call | solution.py:78
  20.2 14.3 %shard_map.182 = f32[1,1024]{1,0:T(1,128)} custom-call(f32[8,1024]{1,0:T(8,128)} %get-tuple-element.10.tail_ref), custom_call_target="tpu_custom_call" | custom-call | tf_op jit(solution)/shard_map/pallas_call | solution.py:132
  34.5 2.0 fusion.16
  36.5 0.3 copy.23
  36.8 4.2 %all_to_all.29 = bf16[2,128,1024]{1,2,0:T(8,128)(2,1)S(1)} all-to-all(bf16[2,128,1024]{1,2,0:T(8,128)(2,1)S(1)} %copy.23), channel_id=1, replica_groups=mesh['sp'=16,'tp'=2] {'tp'}, dimensions={0} | all-to-all | bytes 1048576 | tf_op jit(solution)/shard_map/all_to_all | solution.py:184
  41.0 4.8 %fusion.36 = (f32[128]{0:T(128)S(1)}, f32[128,2048]{1,0:T(8,128)S(1)}) fusion(bf16[128,2048]{0,1:T(8,128)(2,1)S(1)} %bitcast.38, bf16[2048,2048]{1,0:T(8,128)(2,1)} %param.26, bf16[128,2048]{1,0:T(8,128)(2,1)} %param.27), kind=kOutput, calls=%fused_computation.66 | convolution fusion | flops 1074790272 | bytes 10486272 | tf_op jit(solution)/shard_map/dot_general | solution.py:185
  45.8 0.3 multiply_reduce_fusion.2
  46.1 0.2 multiply_convert_fusion.2
  46.4 6.0 %gather_fusion = bf16[1024,2048]{1,0:T(8,128)(2,1)} fusion(bf16[129,2048]{1,0:T(8,128)(2,1)S(1)} %concatenate.10, s32[1024]{0:T(1024)S(1)} %fusion.28), kind=kCustom, calls=%fused_computation | custom fusion | bytes 8392704 | tf_op jit(solution)/shard_map/gather | solution.py:209
  52.4 102.3 %all_to_all.30 = bf16[32,32,2048]{2,1,0:T(8,128)(2,1)S(1)} all-to-all(bf16[32,32,2048]{2,1,0:T(8,128)(2,1)} %bitcast.34), channel_id=1, replica_groups=mesh['sp'=16,'tp'=2] {'sp','tp'}, dimensions={0} | all-to-all | bytes 8388608 | tf_op jit(solution)/shard_map/all_to_all | solution.py:215
  154.7 2.0 copy-done.2
  156.7 3.7 %fusion.2 = f32[1024,512]{1,0:T(8,128)} fusion(bf16[1024,2048]{1,0:T(8,128)(2,1)S(1)} %bitcast.36, bf16[1,2048,512]{2,1,0:T(8,128)(2,1)S(1)} %copy-done.7), kind=kOutput, calls=%fused_computation.9 | convolution fusion | flops 2147483648 | bytes 8388608 | tf_op jit(solution)/shard_map/dot_general | solution.py:221
  160.4 10.1 %convolution_convert_fusion = bf16[1024,2048]{1,0:T(8,128)(2,1)} fusion(bf16[1,512,2048]{2,1,0:T(8,128)(2,1)S(1)} %copy-done, f32[1024,512]{1,0:T(8,128)} %fusion.2, bf16[1024,2048]{1,0:T(8,128)(2,1)} %bitcast.37, bf16[1,2048,512]{2,1,0:T(8,128)(2,1)} %param.34), kind=kOutput, calls=%fused_computation.4 | convolution fusion | flops 4300210176 | bytes 14680064 | tf_op jit(solution)/shard_map/dot_general | solution.py:224
  170.5 4.0 %all-to-all-start.2 = ((bf16[32,32,2048]{2,1,0:T(8,128)(2,1)}), bf16[32,32,2048]{2,1,0:T(8,128)(2,1)}, u32[]{:S(2)}, u32[]{:S(2)}) async-start(bf16[32,32,2048]{2,1,0:T(8,128)(2,1)} %bitcast.35), calls=%async_computation.2 | async-start | bytes 8388608 | tf_op jit(solution)/shard_map/all_to_all | solution.py:223
  174.6 2.0 fusion.38
  176.6 91.5 %all-to-all-done.2 = bf16[32,32,2048]{2,1,0:T(8,128)(2,1)} async-done(((bf16[32,32,2048]{2,1,0:T(8,128)(2,1)}), bf16[32,32,2048]{2,1,0:T(8,128)(2,1)}, u32[]{:S(2)}, u32[]{:S(2)}) %all-to-all-start.2) | async-done | bytes 4194336 | tf_op jit(solution)/shard_map/all_to_all | solution.py:223
  268.1 8.0 %gather_fusion.1 = bf16[512,2048]{1,0:T(8,128)(2,1)} fusion(bf16[1024,2048]{1,0:T(8,128)(2,1)} %bitcast.13, s32[1024]{0:T(1024)S(1)} %pad_clamp_fusion), kind=kCustom, calls=%fused_computation.1 | custom fusion | bytes 4196352 | tf_op jit(solution)/shard_map/gather | solution.py:232
  276.1 4.8 %reshape.87 = f32[128,4,2048]{2,1,0:T(4,128)} reshape(bf16[512,2048]{1,0:T(8,128)(2,1)} %gather_fusion.1) | data formatting | bytes 6291456 | tf_op jit(solution)/shard_map/convert_element_type | solution.py:235
  280.8 6.3 %multiply_reduce_fusion = f32[128,2048]{1,0:T(8,128)} fusion(f32[128,4,2048]{2,1,0:T(4,128)} %reshape.87, f32[128,4]{1,0:T(8,128)S(1)} %copy.24), kind=kLoop, calls=%fused_computation.3 | loop fusion | flops 1835008 | bytes 5244928 | tf_op jit(solution)/shard_map/reduce_sum | solution.py:235
  287.2 3.8 %fusion.37 = (f32[128]{0:T(128)S(1)}, f32[128,2048]{1,0:T(8,128)S(1)}) fusion(f32[128,2048]{1,0:T(8,128)} %multiply_reduce_fusion, bf16[512,2048]{1,0:T(8,128)(2,1)} %param.33, bf16[128,2048]{1,0:T(8,128)(2,1)} %copy-done.1, bf16[2048,512]{1,0:T(8,128)(2,1)} %param.32, f32[128,512]{1,0:T(8,128)S(1)} %fusion.38), kind=kOutput, calls=%fused_computation.67 | convolution fusion | flops 538574720 | bytes 7078400 | tf_op jit(solution)/shard_map/dot_general | solution.py:214
  291.0 0.3 multiply_reduce_fusion.1
  291.2 1.0 multiply_convert_fusion.1
  (29 shorter events, 0.5 us)
Async XLA Ops:
  0.0 160.4 %copy-start = (bf16[1,512,2048]{2,1,0:T(8,128)(2,1)S(1)}, bf16[1,512,2048]{2,1,0:T(8,128)(2,1)}, u32[]{:S(2)}) copy-start(bf16[1,512,2048]{2,1,0:T(8,128)(2,1)} %param.36) | copy-start | bytes 6291460
  0.0 34.5 %copy-start.3 = (bf16[256,1024]{1,0:T(8,128)(2,1)S(1)}, bf16[256,1024]{1,0:T(8,128)(2,1)}, u32[]{:S(2)}) copy-start(bf16[256,1024]{1,0:T(8,128)(2,1)} %param.19) | copy-start | bytes 1572868
  0.9 12.2 %collective-permute-start = (bf16[3,1024]{1,0:T(4,128)(2,1)S(1)}, bf16[3,1024]{1,0:T(4,128)(2,1)S(1)}, u32[]{:S(2)}, u32[]{:S(2)}) collective-permute-start(bf16[3,1024]{1,0:T(4,128)(2,1)S(1)} %slice.3), channel_id=1, source_target_pairs={{0,2},{2,4},{4,6},{6,8},{8,10},{10,12},{12,14},{14,16},{16,18},{18... | collective-permute-start | bytes 18440 | tf_op jit(solution)/shard_map/ppermute | solution.py:19
  41.0 5.1 %copy-start.4 = (f32[2048]{0:T(1024)S(1)}, f32[2048]{0:T(1024)}, u32[]{:S(2)}) copy-start(f32[2048]{0:T(1024)} %param.28) | copy-start | bytes 24580
  46.3 128.3 %copy-start.1 = (bf16[128,2048]{1,0:T(8,128)(2,1)}, bf16[128,2048]{1,0:T(8,128)(2,1)S(1)}, u32[]{:S(2)}) copy-start(bf16[128,2048]{1,0:T(8,128)(2,1)S(1)} %multiply_convert_fusion.2) | copy-start | bytes 1572868
  52.4 104.3 %copy-start.7 = (bf16[1,2048,512]{2,1,0:T(8,128)(2,1)S(1)}, bf16[1,2048,512]{2,1,0:T(8,128)(2,1)}, u32[]{:S(2)}) copy-start(bf16[1,2048,512]{2,1,0:T(8,128)(2,1)} %param.35) | copy-start | bytes 6291460
  154.7 2.0 copy-start.2
  170.5 4.0 %copy-start.6 = (f32[128,4]{0,1:T(4,128)S(1)}, f32[128,4]{0,1:T(4,128)}, u32[]{:S(2)}) copy-start(f32[128,4]{0,1:T(4,128)} %param.30) | copy-start | bytes 6148
  170.5 97.7 %all-to-all-start.2 = ((bf16[32,32,2048]{2,1,0:T(8,128)(2,1)}), bf16[32,32,2048]{2,1,0:T(8,128)(2,1)}, u32[]{:S(2)}, u32[]{:S(2)}) async-start(bf16[32,32,2048]{2,1,0:T(8,128)(2,1)} %bitcast.35), calls=%async_computation.2 | async-start | bytes 8388608 | tf_op jit(solution)/shard_map/all_to_all | solution.py:223
  287.2 4.1 %copy-start.5 = (f32[2048]{0:T(1024)S(1)}, f32[2048]{0:T(1024)}, u32[]{:S(2)}) copy-start(f32[2048]{0:T(1024)} %param.37) | copy-start | bytes 24580

commit v2 on v1

--- a/solution.py
+++ b/solution.py
@@ -149,6 +149,200 @@
     return center * lax.rsqrt(spread + NORM_EPS) * gains
 
 
+def experts_kernel(
+    outer,
+    inner,
+    cores,
+    capacity,
+    rows_ref,
+    meta_ref,
+    shared_gate_ref,
+    shared_up_ref,
+    shared_down_ref,
+    gate_ref,
+    up_ref,
+    down_ref,
+    out_ref,
+    rows,
+    meta,
+    packed,
+    arrived,
+    result,
+    back,
+    part,
+    part_land,
+    row_sems,
+    meta_sems,
+    go_sems,
+    back_sems,
+    part_sems,
+):
+    sp, core = lax.axis_index("sp"), lax.axis_index("tp")
+    layer, place = sp // inner, lax.rem(sp, inner) * cores + core
+    plane = inner * cores
+    slots = plane * capacity
+    fanout = meta_ref.shape[0] // 2
+
+    def along(d):
+        return (lax.rem(layer + d + outer, outer) * inner + lax.rem(sp, inner), core)
+
+    def across(d):
+        other = lax.rem(place + d + plane, plane)
+        return (layer * inner + other // cores, lax.rem(other, cores))
+
+    def remote(src, dst, sems, index, device):
+        return pltpu.make_async_remote_copy(
+            src_ref=src,
+            dst_ref=dst,
+            send_sem=sems.at[(0, *index)],
+            recv_sem=sems.at[(1, *index)],
+            device_id=device,
+            device_id_type=MESH,
+        )
+
+    def row_copy(d):
+        return remote(rows_ref, rows.at[d], row_sems, (d,), along(d))
+
+    def meta_copy(d):
+        return remote(meta_ref, meta.at[d], meta_sems, (d,), along(d))
+
+    def piece(ref, b, d):
+        return ref.at[b, pl.ds(d * capacity, capacity)]
+
+    def go_copy(b, d):
+        return remote(piece(packed, b, d), piece(arrived, b, d), go_sems, (b, d), across(d))
+
+    def back_copy(b, d):
+        return remote(piece(result, b, d), piece(back, b, d), back_sems, (b, d), across(-d))
+
+    def part_copy(b):
+        return remote(part.at[b], part_land.at[b], part_sems, (b,), along(-b))
+
+    barrier = pltpu.get_barrier_semaphore()
+    for d in range(1, outer):
+        pl.semaphore_signal(barrier, inc=1, device_id=along(d), device_id_type=MESH)
+    for d in range(1, plane):
+        pl.semaphore_signal(barrier, inc=1, device_id=across(d), device_id_type=MESH)
+    pl.semaphore_wait(barrier, outer + plane - 2)
+    for d in range(1, outer):
+        meta_copy(d).start()
+        row_copy(d).start()
+    rows[0] = rows_ref[...]
+    meta[0] = meta_ref[...]
+
+    def wanted(b):
+        width = meta_ref.shape[1]
+        slot = lax.broadcasted_iota(jnp.int32, (slots, width), 0) + place * capacity
+        slot = jnp.where(slot >= slots, slot - slots, slot) + layer * slots
+        return slot.astype(jnp.float32)
+
+    def weighed(b, ones):
+        slot = wanted(b)
+        total = jnp.zeros(slot.shape, jnp.float32)
+        for k in range(fanout):
+            value = 1.0 if ones else meta[b, fanout + k : fanout + k + 1]
+            total = total + jnp.where(slot == meta[b, k : k + 1], value, 0.0)
+        return total
+
+    def pack(b):
+        chosen = jnp.dot(
+            weighed(b, True).astype(jnp.bfloat16), rows[b], preferred_element_type=jnp.float32
+        ).astype(jnp.bfloat16)
+        packed[b] = chosen
+        arrived[b, :capacity] = chosen[:capacity]
+        for d in range(1, plane):
+            go_copy(b, d).start()
+
+    def gated(x, gate, up, down):
+        hidden = (
+            jax.nn.silu(jnp.dot(x, gate, preferred_element_type=jnp.float32))
+            * jnp.dot(x, up, preferred_element_type=jnp.float32)
+        ).astype(jnp.bfloat16)
+        return jnp.dot(hidden, down, preferred_element_type=jnp.float32)
+
+    pack(0)
+    out_ref[...] = gated(rows_ref[...], shared_gate_ref[...], shared_up_ref[...], shared_down_ref[...])
+
+    def turn(step, carry):
+        @pl.when(step < outer)
+        def _():
+            meta_copy(step).wait()
+            row_copy(step).wait()
+            pack(step)
+
+        @pl.when(step <= outer)
+        def _():
+            b = step - 1
+            for d in range(1, plane):
+                go_copy(b, d).wait()
+            done = gated(arrived[b], gate_ref[0], up_ref[0], down_ref[0]).astype(jnp.bfloat16)
+            result[b] = done
+            back[b, :capacity] = done[:capacity]
+            for d in range(1, plane):
+                back_copy(b, d).start()
+
+        @pl.when(step >= 2)
+        def _():
+            b = step - 2
+            for d in range(1, plane):
+                back_copy(b, d).wait()
+            weight = weighed(b, False).T
+            high = weight.astype(jnp.bfloat16)
+            low = (weight - high.astype(jnp.float32)).astype(jnp.bfloat16)
+            summed = jnp.dot(high, back[b], preferred_element_type=jnp.float32) + jnp.dot(
+                low, back[b], preferred_element_type=jnp.float32
+            )
+
+            @pl.when(b == 0)
+            def _():
+                out_ref[...] += summed
+
+            @pl.when(b > 0)
+            def _():
+                part[b] = summed.astype(jnp.bfloat16)
+                part_copy(b).start()
+
+        return carry
+
+    lax.fori_loop(1, outer + 2, turn, 0)
+    for b in range(1, outer):
+        part_copy(b).wait()
+        out_ref[...] += part_land[b].astype(jnp.float32)
+
+
+def experts_sum(normed, meta, capacity, weights):
+    sp_count, cores = lax.axis_size("sp"), lax.axis_size("tp")
+    outer = 4 if sp_count % 4 == 0 else 1
+    inner = sp_count // outer
+    plane = inner * cores
+    rows, width = normed.shape
+    bf16 = lambda *shape: pltpu.VMEM((*shape, width), jnp.bfloat16)
+    sems = lambda *shape: pltpu.SemaphoreType.DMA((2, *shape))
+    slots = plane * capacity
+    return pl.pallas_call(
+        functools.partial(experts_kernel, outer, inner, cores, capacity),
+        out_shape=jax.ShapeDtypeStruct((rows, width), jnp.float32),
+        in_specs=[pl.BlockSpec(memory_space=pltpu.VMEM)] * 8,
+        out_specs=pl.BlockSpec(memory_space=pltpu.VMEM),
+        scratch_shapes=[
+            bf16(outer, rows),
+            pltpu.VMEM((outer, *meta.shape), jnp.float32),
+            bf16(outer, slots),
+            bf16(outer, slots),
+            bf16(outer, slots),
+            bf16(outer, slots),
+            bf16(outer, rows),
+            bf16(outer, rows),
+            sems(outer),
+            sems(outer),
+            sems(outer, plane),
+            sems(outer, plane),
+            sems(outer),
+        ],
+        compiler_params=pltpu.CompilerParams(collective_id=1, has_side_effects=True),
+    )(normed, meta, *weights)
+
+
 def on_device(
     gate_pre,
     conv_in,
@@ -186,7 +380,6 @@
     normed = layer_norm(ALPHA * residual.astype(jnp.float32) + projected, gain_mix).astype(
         jnp.bfloat16
     )
-    model_width = normed.shape[1]
     fanout = routes.shape[1]
     sp_count, tp_count = (lax.axis_size("sp"), lax.axis_size("tp"))
     experts = sp_count * tp_count
@@ -200,39 +393,15 @@
     earlier = jnp.dot(before_mask, onehot, preferred_element_type=jnp.float32)
     slot_rank = jnp.sum(earlier * onehot.astype(jnp.float32), axis=1).astype(jnp.int32)
     slot_index = flat_ids * capacity + slot_rank
-    source_row = (
-        jnp.full((experts * capacity,), row_count, jnp.int32)
-        .at[slot_index]
-        .set(lax.iota(jnp.int32, entries) // fanout)
+    meta = jnp.concatenate(
+        [slot_index.reshape(row_count, fanout).T.astype(jnp.float32), route_weight.T], axis=0
     )
-    padded_rows = jnp.concatenate([normed, jnp.zeros((1, model_width), jnp.bfloat16)], axis=0)
-    outgoing = padded_rows[source_row].reshape(experts, capacity, model_width)
-    shared_hidden = (
-        jax.nn.silu(jnp.dot(normed, shared_gate, preferred_element_type=jnp.float32))
-        * jnp.dot(normed, shared_up, preferred_element_type=jnp.float32)
-    ).astype(jnp.bfloat16)
-    shared_out = jnp.dot(shared_hidden, shared_down, preferred_element_type=jnp.float32)
-    received = lax.all_to_all(outgoing, ("sp", "tp"), split_axis=0, concat_axis=0, tiled=True)
-    senders = received.shape[0]
-    slot_count = received.shape[1]
-    chosen = received.reshape(senders * slot_count, model_width)
-    hidden = (
-        jax.nn.silu(jnp.dot(chosen, expert_gate[0], preferred_element_type=jnp.float32))
-        * jnp.dot(chosen, expert_up[0], preferred_element_type=jnp.float32)
-    ).astype(jnp.bfloat16)
-    handed_result = lax.all_to_all(
-        jnp.dot(hidden, expert_down[0], preferred_element_type=jnp.float32)
-        .astype(jnp.bfloat16)
-        .reshape(senders, slot_count, model_width),
-        ("sp", "tp"),
-        split_axis=0,
-        concat_axis=0,
-        tiled=True,
+    moe_sum = experts_sum(
+        normed,
+        meta,
+        capacity,
+        (shared_gate, shared_up, shared_down, expert_gate, expert_up, expert_down),
     )
-    gathered = handed_result.reshape(experts * capacity, model_width)[slot_index].reshape(
-        row_count, fanout, model_width
-    )
-    moe_sum = shared_out + jnp.sum(route_weight[:, :, None] * gathered.astype(jnp.float32), axis=1)
     return layer_norm(ALPHA * normed.astype(jnp.float32) + moe_sum, gain_out).astype(jnp.bfloat16)
 
 

time: 293 us -> 184 us (0.63)
  Pallas kernels: 20.8 us -> 154 us
  blocking collectives: 106 us -> 4.15 us
  waiting for transfers between devices: 91.5 us -> 0.01 us
  local copies, waits for them, and re-layouts: 27.1 us -> 3.61 us
  matrix products: 24.7 us -> 5.04 us
  starting transfers between devices: 8.83 us -> 4.86 us
    pallas_call x0 -> x1, Pallas kernels: none -> 133 us  [experts_sum(): pl.pallas_call(functools.partial(experts_kernel, outer, inner, cores, cap...]
    all_to_all x1 -> x0, blocking collectives: 102 us -> none  [on_device(): lax.all_to_all(outgoing, ('sp', 'tp'), split_axis=0, concat_axis=0, tiled...]
    all_to_all x1 -> x0, waiting for transfers between devices: 91.5 us -> none  [on_device(): lax.all_to_all(jnp.dot(hidden, expert_down[0], preferred_element_type=jnp...]
    dot_general x4 -> x0, matrix products: 19.6 us -> none  [the longest x1 10.1 us: on_device(): jnp.dot(hidden, expert_down[0], preferred_element_type=jnp.float32)]
    gather x2 -> x0, local copies, waits for them, and re-layouts: 14 us -> none  [the longest x1 7.96 us: on_device(): handed_result.reshape(experts * capacity, model_width)[slot_index]]
    reduce_sum x1, other arithmetic: 6.33 us -> 1.66 us  [layer_norm(): center = values - jnp.mean(values, axis=-1, keepdims=True)]
    convert_element_type x1 -> x2, local copies, waits for them, and re-layouts: 4.75 us -> 0.16 us  [on_device(): jnp.sum(earlier * onehot.astype(jnp.float32), axis=1).astype(jnp.int32)]
    all_to_all x1 -> x0, starting transfers between devices: 3.97 us -> none  [on_device(): lax.all_to_all(jnp.dot(hidden, expert_down[0], preferred_element_type=jnp...]
  transfers between devices with their start and end apart: 2 -> 1, of which waited for: 1 -> 0; matrix products, arithmetic and copies ran while one was open for 3% -> 3% of each run, Pallas kernels for 0% -> 0%
where the time goes in v2:
time: 184 us; the launch traced here: 183 us
  Pallas kernels  154 us (84%)
  other arithmetic  10.7 us (6%)
  matrix products  5.04 us (3%)
  starting transfers between devices  4.86 us (3%)
  blocking collectives  4.15 us (2%)
  local copies, waits for them, and re-layouts  3.61 us (2%)
    pallas_call x1, Pallas kernels, experts_sum(): pl.pallas_call(functools.partial(experts_kernel, outer, inner, cores, cap...  133 us
    pallas_call x1, Pallas kernels, entering(): pl.pallas_call(functools.partial(entering_kernel, count), out_shape=jax.S...  14.3 us
    pallas_call x1, Pallas kernels, recurrence(): pl.pallas_call(recurrence_kernel, grid=(heads,), in_specs=[pl.BlockSpec((...  6.44 us
    ppermute x1, starting transfers between devices, from_behind(): return lax.ppermute(block, axis, route)  4.86 us
    dot_general x1, matrix products, on_device(): jnp.dot(regrouped, out_weight, preferred_element_type=jnp.float32)  4.76 us
    all_to_all x1, blocking collectives, on_device(): lax.all_to_all(mixed_rows, 'tp', split_axis=0, concat_axis=1, tiled=True)  4.15 us
  transfers between devices with their start and end apart: 1, of which 0 were waited for; matrix products, arithmetic and copies ran while one was open for 3% of the time, Pallas kernels for 0%

profile of v2, /device:TPU:0, one launch (start us, length us, event | category | flops | bytes accessed | tf_op | source)
XLA Modules:
  0.0 182.5 jit_solution(10875155785478086619)
XLA Ops:
  0.0 0.8 slice.3
  0.8 4.9 %collective-permute-start = (bf16[3,1024]{1,0:T(4,128)(2,1)S(1)}, bf16[3,1024]{1,0:T(4,128)(2,1)S(1)}, u32[]{:S(2)}, u32[]{:S(2)}) collective-permute-start(bf16[3,1024]{1,0:T(4,128)(2,1)S(1)} %slice.3), channel_id=1, source_target_pairs={{0,2},{2,4},{4,6},{6,8},{8,10},{10,12},{12,14},{14,16},{16,18},{18... | collective-permute-start | bytes 18440 | tf_op jit(solution)/shard_map/ppermute | solution.py:19
  5.7 1.3 fusion.11
  6.9 0.8 copy.23
  7.7 0.1 eq.15
  7.8 0.3 fusion
  8.1 0.1 convert_element_type.47
  8.2 0.1 copy.24
  8.3 0.7 convert_bitcast_fusion
  9.0 1.3 pad_maximum_fusion.meta_ref
  10.3 1.5 copy.21.shift_ref
  11.8 0.0 collective-permute-done
  11.8 0.6 pad_convert_fusion.before_ref
  12.4 6.4 %shard_map.181 = (f32[256,1024]{1,0:T(8,128)}, f32[256,1024]{1,0:T(8,128)}, f32[8,1024]{1,0:T(8,128)}) custom-call(f32[8,1024]{1,0:T(8,128)} %pad_convert_fusion.before_ref, bf16[256,1024]{1,0:T(8,128)(2,1)} %conv_ref.1, bf16[4,1024]{1,0:T(4,128)(2,1)} %taps_ref.1, bf16[4,256,256]{2,1,0:T(8,128)(2,1)} %recur_ref.1, bf16[4,256,256]{2,1,0:T(8,128)(2,1)} %input_ref.1, ...), custom_call_target="tpu_custom_call" | custom-call | tf_op jit(solution)/shard_map/pallas_call | solution.py:78
  18.8 14.3 %shard_map.182 = f32[1,1024]{1,0:T(1,128)} custom-call(f32[8,1024]{1,0:T(8,128)} %get-tuple-element.10.tail_ref), custom_call_target="tpu_custom_call" | custom-call | tf_op jit(solution)/shard_map/pallas_call | solution.py:132
  33.2 0.0 copy-done.2
  33.2 0.0 copy-start.1
  33.2 2.1 %fusion.7 = bf16[256,1024]{1,0:T(8,128)(2,1)S(1)} fusion(bf16[256,1024]{1,0:T(8,128)(2,1)S(1)} %copy-done.2, f32[256,1024]{1,0:T(8,128)} %get-tuple-element.8, f32[256,1024]{1,0:T(8,128)} %get-tuple-element.9, f32[1024]{0:T(1024)} %bitcast.13), kind=kLoop, calls=%fused_computation.13 | loop fusion | flops 3407872 | bytes 3149824 | tf_op jit(solution)/shard_map/convert_element_type | solution.py:376
  35.3 0.3 copy.22
  35.5 4.2 %all_to_all.19 = bf16[2,128,1024]{1,2,0:T(8,128)(2,1)S(1)} all-to-all(bf16[2,128,1024]{1,2,0:T(8,128)(2,1)S(1)} %copy.22), channel_id=1, replica_groups=mesh['sp'=16,'tp'=2] {'tp'}, dimensions={0} | all-to-all | bytes 1048576 | tf_op jit(solution)/shard_map/all_to_all | solution.py:378
  39.7 0.0 copy-done.1
  39.7 4.8 %fusion.12 = (f32[128]{0:T(128)S(1)}, f32[128,2048]{1,0:T(8,128)S(1)}) fusion(bf16[128,2048]{0,1:T(8,128)(2,1)S(1)} %bitcast.11, bf16[2048,2048]{1,0:T(8,128)(2,1)} %param.26, bf16[128,2048]{1,0:T(8,128)(2,1)S(1)} %copy-done.1), kind=kOutput, calls=%fused_computation.33 | convolution fusion | flops 1074790272 | bytes 10486272 | tf_op jit(solution)/shard_map/dot_general | solution.py:379
  44.5 0.3 multiply_reduce_fusion.1
  44.7 0.0 copy-done.3
  44.8 1.0 multiply_convert_fusion.1.rows_ref
  45.8 133.3 %shard_map.183 = f32[128,2048]{1,0:T(8,128)} custom-call(bf16[128,2048]{1,0:T(8,128)(2,1)} %multiply_convert_fusion.1.rows_ref, f32[8,128]{1,0:T(8,128)} %pad_maximum_fusion.meta_ref, bf16[2048,512]{1,0:T(8,128)(2,1)} %shared_gate_ref.1, bf16[2048,512]{1,0:T(8,128)(2,1)} %shared_up_ref.1, bf16[512,2048]{1,0:T(8,128)(2,1)} %shared_down_ref.1, ...), custom_call_target="tpu_custom_call" | custom-call | tf_op jit(solution)/shard_map/pallas_call | solution.py:322
  179.0 0.0 copy-start
  179.1 0.0 copy-start.4
  179.1 1.7 fusion.8
  180.7 0.0 copy-done
  180.7 0.4 multiply_reduce_fusion
  181.2 1.3 multiply_convert_fusion
  (8 shorter events, 0.0 us)
Async XLA Ops:
  0.0 33.2 %copy-start.2 = (bf16[256,1024]{1,0:T(8,128)(2,1)S(1)}, bf16[256,1024]{1,0:T(8,128)(2,1)}, u32[]{:S(2)}) copy-start(bf16[256,1024]{1,0:T(8,128)(2,1)} %param.19) | copy-start | bytes 1572868
  0.8 11.0 %collective-permute-start = (bf16[3,1024]{1,0:T(4,128)(2,1)S(1)}, bf16[3,1024]{1,0:T(4,128)(2,1)S(1)}, u32[]{:S(2)}, u32[]{:S(2)}) collective-permute-start(bf16[3,1024]{1,0:T(4,128)(2,1)S(1)} %slice.3), channel_id=1, source_target_pairs={{0,2},{2,4},{4,6},{6,8},{8,10},{10,12},{12,14},{14,16},{16,18},{18... | collective-permute-start | bytes 18440 | tf_op jit(solution)/shard_map/ppermute | solution.py:19
  33.2 6.5 %copy-start.1 = (bf16[128,2048]{1,0:T(8,128)(2,1)S(1)}, bf16[128,2048]{1,0:T(8,128)(2,1)}, u32[]{:S(2)}) copy-start(bf16[128,2048]{1,0:T(8,128)(2,1)} %param.27) | copy-start | bytes 1572868
  39.7 5.0 %copy-start.3 = (f32[2048]{0:T(1024)S(1)}, f32[2048]{0:T(1024)}, u32[]{:S(2)}) copy-start(f32[2048]{0:T(1024)} %param.28) | copy-start | bytes 24580
  179.0 1.7 copy-start
  179.1 2.1 %copy-start.4 = (f32[2048]{0:T(1024)S(1)}, f32[2048]{0:T(1024)}, u32[]{:S(2)}) copy-start(f32[2048]{0:T(1024)} %param.37) | copy-start | bytes 24580
